TPU v7x, 32 devices: a whole 2x2x4 slice. The times are simulated.
32 devices in a mesh: fs: 8 (over z, x), tp: 4 (over y, core).
Axes of the slice: x: 2, y: 2, z: 4, core: 2. Of those that a mesh axis runs over, the one named last changes fastest.
Arguments:
- tokens: bfloat16 [64, 2048], P(('fs', 'tp')), may hold values from -6 to 6
- route_experts: int32 [64, 2], P(('fs', 'tp')), may hold values from 0 to 3, as said below
- route_logits: float32 [64, 2], P(('fs', 'tp')), may hold values from -8 to 8
- norm_gain: float32 [2048], P('fs'), may hold values from 0.1 to 1.9
- gate_train: float32 [4, 2048, 8192], P(None, 'fs', 'tp'), may hold values from -0.125 to 0.125
- up_train: float32 [4, 2048, 8192], P(None, 'fs', 'tp'), may hold values from -0.125 to 0.125
- down_train: float32 [4, 2048, 8192], P(None, 'fs', 'tp'), may hold values from -0.125 to 0.125
Outputs:
- gate_serve: bfloat16 [8, 2048, 4096], P('fs')
- up_serve: bfloat16 [8, 2048, 4096], P('fs')
- down_serve: bfloat16 [8, 2048, 4096], P('fs')
- mixed: bfloat16 [64, 2048], P(('fs', 'tp'))
Inputs may be any that keep to these rules, and one draw needn't show every extreme that they name: `route_experts`: the two experts of a row differ; any expert may be named by every row of the devices that share one index along tp, and in every draw some expert is.
All inputs are finite; a program needn't handle non-finite values.
Results may differ from a plain program's by a relative error of at most 0.0085.
Values may be sent and summed in bfloat16 or wider, within the bound.
A program may use at most 192 MiB of HBM per device.

v0:
```python
import functools

import jax
import jax.numpy as jnp
from jax import lax
from jax.experimental import pallas as pl
from jax.experimental.pallas import tpu as pltpu
from jax.sharding import PartitionSpec as P

MESH = pl.DeviceIdType.MESH
PARTS = 4
LAG_TP = 3
LAG_FS = 6
PAD = 128


def for_sending(array):
    return jax.tree.map(lambda a: a.astype(jnp.bfloat16) if a.dtype == jnp.float32 else a, array)


def normalize(tokens):
    values = tokens.astype(jnp.float32)
    row_mean = jnp.mean(values, axis=-1, keepdims=True)
    centered = values - row_mean
    row_var = jnp.mean(centered * centered, axis=-1, keepdims=True)
    return (centered * lax.rsqrt(row_var + 1e-05)).astype(jnp.bfloat16)


def per_device_general(tokens, route_experts, route_logits, norm_gain, gate_train, up_train, down_train):
    fs_size = lax.axis_size("fs")
    tp_size = lax.axis_size("tp")
    expert_count = gate_train.shape[0]
    slices = fs_size // expert_count
    scale = norm_gain[None, :, None]
    gate_half = (scale * gate_train).astype(jnp.bfloat16)
    up_half = (scale * up_train).astype(jnp.bfloat16)
    down_half = down_train.astype(jnp.bfloat16)
    swapped = (
        lax.all_to_all(gate_half, "tp", split_axis=1, concat_axis=2, tiled=True),
        lax.all_to_all(up_half, "tp", split_axis=1, concat_axis=2, tiled=True),
        lax.all_to_all(down_half, "tp", split_axis=1, concat_axis=2, tiled=True),
    )
    quarter = swapped[0].shape[1]
    hidden_total = swapped[0].shape[2]
    block_width = hidden_total // slices

    def split_quarter(matrix):
        blocks = matrix.reshape(expert_count, quarter, slices, block_width)
        return blocks.transpose(0, 2, 1, 3).reshape(expert_count * slices, quarter, block_width)

    owned = lax.all_to_all(
        for_sending(tuple((split_quarter(matrix) for matrix in swapped))),
        "fs",
        split_axis=0,
        concat_axis=1,
        tiled=True,
    )
    stacked = tuple((matrix.reshape(1, fs_size, 1, quarter, block_width) for matrix in owned))
    joined = jax.tree.map(
        lambda part, own: part.astype(own.dtype),
        lax.all_gather(for_sending(stacked), "tp", axis=2, tiled=True),
        stacked,
    )
    gate_serve, up_serve, down_serve = tuple(
        (matrix.reshape(1, fs_size * tp_size * quarter, block_width) for matrix in joined)
    )
    normed = normalize(tokens)
    first = jax.nn.sigmoid(route_logits[:, 0] - route_logits[:, 1])
    second = jax.nn.sigmoid(route_logits[:, 1] - route_logits[:, 0])
    labels = jnp.arange(expert_count, dtype=jnp.int32)
    table = first[:, None] * (route_experts[:, 0:1] == labels[None, :]).astype(jnp.float32)
    table = table + second[:, None] * (route_experts[:, 1:2] == labels[None, :]).astype(jnp.float32)
    table = table.astype(jnp.bfloat16)
    rows_all, table_all = (
        lax.all_gather(normed, "fs", axis=0, tiled=True),
        lax.all_gather(table, "fs", axis=0, tiled=True),
    )
    own_expert = lax.axis_index("fs") // slices
    selector = (labels == own_expert).astype(jnp.float32)
    weight = jnp.sum(table_all.astype(jnp.float32) * selector[None, :], axis=1)
    gate_act = jnp.dot(rows_all, gate_serve[0], preferred_element_type=jnp.float32)
    up_act = jnp.dot(rows_all, up_serve[0], preferred_element_type=jnp.float32)
    hidden = (weight[:, None] * jax.nn.silu(gate_act) * up_act).astype(jnp.bfloat16)
    down_own = down_serve[0]
    summed = lax.psum_scatter(
        lax.dot_general(
            hidden, down_own, (((1,), (1,)), ((), ())), preferred_element_type=jnp.float32
        ),
        "fs",
        scatter_dimension=0,
        tiled=True,
    )
    return (gate_serve, up_serve, down_serve, summed.astype(jnp.bfloat16))


def round_kernel(gain_ref, gate_ref, up_ref, down_ref, out_ref):
    gain = gain_ref[...]
    out_ref[0, 0] = (gain * gate_ref[0]).astype(jnp.bfloat16)
    out_ref[1, 0] = (gain * up_ref[0]).astype(jnp.bfloat16)
    out_ref[2, 0] = down_ref[0].astype(jnp.bfloat16)


def rounded(norm_gain, gate_train, up_train, down_train):
    experts, rows, width = gate_train.shape
    tile = rows // 2
    weight = pl.BlockSpec((1, tile, width), lambda e, r: (e, r, 0))
    return pl.pallas_call(
        round_kernel,
        grid=(experts, rows // tile),
        in_specs=[pl.BlockSpec((tile, 1), lambda e, r: (r, 0)), weight, weight, weight],
        out_specs=pl.BlockSpec((3, 1, tile, width), lambda e, r: (0, e, r, 0)),
        out_shape=jax.ShapeDtypeStruct((3, experts, rows, width), jnp.bfloat16),
        name="round_weights",
    )(norm_gain[:, None], gate_train, up_train, down_train)


def exchange_kernel(
    src, mine_ref, joined, transit, all_ref, held, l_in, l_out, z_s, z_r, y_s, y_r, x_s, x_r,
    c_s, c_r, g_s, g_r
):
    matrices, experts, rows, width = src.shape
    chunk = rows // PARTS
    pieces = matrices * PARTS * experts
    f = lax.axis_index("fs")
    t = lax.axis_index("tp")
    z, x = lax.div(f, 2), lax.rem(f, 2)
    s, c = lax.div(t, 2), lax.rem(t, 2)
    y_peer = (f, (1 - s) * 2 + c)
    c_peer = (f, s * 2 + 1 - c)
    x_peer = (z * 2 + 1 - x, t)

    def z_peer(d):
        return (lax.rem(z + d, experts) * 2 + x, t)

    barrier = pltpu.get_barrier_semaphore()
    fs_size = all_ref.shape[0]
    fs_peers = [(lax.rem(f + q, fs_size), t) for q in range(1, fs_size)]
    for peer in (*fs_peers, y_peer, c_peer):
        pl.semaphore_signal(barrier, inc=1, device_id=peer, device_id_type=MESH)

    def parts_of(k):
        d = lax.rem(k, experts)
        g = lax.div(k, experts)
        return d, g, lax.rem(g, PARTS), lax.div(g, PARTS)

    def final(m, zs, xs, h):
        row = pl.multiple_of((zs * 2 + xs) * rows + h * chunk, chunk)
        return joined.at[m, pl.ds(row, chunk), pl.ds(pl.multiple_of(c * width, width), width)]

    def passing(m, zs, h):
        return transit.at[m, zs, pl.ds(pl.multiple_of(h * chunk, chunk), chunk)]

    def source(m, e, h):
        return src.at[m, e, pl.ds(pl.multiple_of(h * chunk, chunk), chunk)]

    def remote(a, b, send, recv, peer):
        return pltpu.make_async_remote_copy(
            src_ref=a, dst_ref=b, send_sem=send, recv_sem=recv, device_id=peer,
            device_id_type=MESH,
        )

    def load(g):
        return pltpu.make_async_copy(
            source(lax.div(g, PARTS), z, lax.rem(g, PARTS)), held.at[g], l_in.at[g]
        )

    @pl.loop(0, matrices * PARTS)
    def _(g):
        load(g).start()

    all_ref[f] = mine_ref[...]
    pl.semaphore_wait(barrier, fs_size + 1)
    for q, peer in enumerate(fs_peers):
        remote(mine_ref, all_ref.at[f], g_s.at[q], g_r.at[q], peer).start()

    def send_z(home):
        @pl.loop(0, pieces)
        def _(k):
            d, g, h, m = parts_of(k)

            @pl.when(d > 0)
            def _():
                here = final(m, z, x, h) if home else passing(m, z, h)
                there = source(m, lax.rem(z + d, experts), h)
                remote(there, here, z_s.at[k], z_r.at[k], z_peer(d)).start()

            @pl.when(d == 0)
            def _():
                here = final(m, z, x, h) if home else passing(m, z, h)
                load(g).wait()
                pltpu.make_async_copy(held.at[g], here, l_out.at[g]).start()

    def place(k, keep):
        d, g, h, m = parts_of(k)
        zs = lax.rem(z + experts - d, experts)
        return final(m, zs, x, h) if keep else passing(m, zs, h)

    def forward(k, keep):
        d, g, h, m = parts_of(k)
        zs = lax.rem(z + experts - d, experts)
        if keep:
            here = final(m, zs, x, h)
            remote(here, here, c_s.at[k], c_r.at[k], c_peer).start()
        else:
            remote(
                passing(m, zs, h), final(m, zs, x, h), x_s.at[k], x_r.at[k], x_peer
            ).start()

    def run(home):
        send_z(home)

        @pl.loop(0, pieces + LAG_FS)
        def _(i):
            @pl.when(i < pieces)
            def _():
                d, g, h, m = parts_of(i)
                here = place(i, home)

                @pl.when(d > 0)
                def _():
                    remote(here, here, z_s.at[i], z_r.at[i], y_peer).wait_recv()

                @pl.when(d == 0)
                def _():
                    pltpu.make_async_copy(held.at[g], here, l_out.at[g]).wait()

                remote(here, here, y_s.at[i], y_r.at[i], y_peer).start()
                forward(i, home)

            @pl.when((i >= LAG_TP) & (i < pieces + LAG_TP))
            def _():
                k = i - LAG_TP
                here = place(k, not home)
                remote(here, here, y_s.at[k], y_r.at[k], y_peer).wait_recv()
                forward(k, not home)

            @pl.when(i >= LAG_FS)
            def _():
                k = i - LAG_FS
                d, g, h, m = parts_of(k)
                here = final(m, lax.rem(z + experts - d, experts), 1 - x, h)
                remote(here, here, x_s.at[k], x_r.at[k], x_peer).wait_recv()
                remote(
                    here, here, c_s.at[pieces + k], c_r.at[pieces + k], c_peer
                ).start()

        @pl.loop(0, pieces)
        def _(k):
            d, g, h, m = parts_of(k)
            zs = lax.rem(z + experts - d, experts)
            here = place(k, home)

            @pl.when(d > 0)
            def _():
                remote(
                    source(m, lax.rem(z + d, experts), h), here, z_s.at[k], z_r.at[k], y_peer
                ).wait_send()

            remote(here, here, y_s.at[k], y_r.at[k], y_peer).wait_send()
            remote(passing(m, zs, h), here, x_s.at[k], x_r.at[k], x_peer).wait_send()
            for q in range(2):
                xs = x if q == 0 else 1 - x
                mine = final(m, zs, xs, h)
                row = pl.multiple_of((zs * 2 + xs) * rows + h * chunk, chunk)
                other = joined.at[
                    m, pl.ds(row, chunk), pl.ds(pl.multiple_of((1 - c) * width, width), width)
                ]
                n = q * pieces + k
                remote(mine, other, c_s.at[n], c_r.at[n], c_peer).wait()

    @pl.when(s == x)
    def _():
        run(True)

    @pl.when(s != x)
    def _():
        run(False)

    for q, peer in enumerate(fs_peers):
        owner = lax.rem(f + fs_size - q - 1, fs_size)
        remote(mine_ref, all_ref.at[owner], g_s.at[q], g_r.at[q], peer).wait()


def exchanged(packed, mine, fs_size):
    matrices, experts, rows, width = packed.shape
    pieces = matrices * PARTS * experts
    groups = matrices * PARTS
    anywhere = pl.BlockSpec(memory_space=pl.ANY)
    in_vmem = pl.BlockSpec(memory_space=pltpu.VMEM)
    dma = pltpu.SemaphoreType.DMA
    return pl.pallas_call(
        exchange_kernel,
        in_specs=[anywhere, in_vmem],
        out_specs=[anywhere, anywhere, in_vmem],
        out_shape=[
            jax.ShapeDtypeStruct((matrices, fs_size * rows, 2 * width), jnp.bfloat16),
            jax.ShapeDtypeStruct(packed.shape, jnp.bfloat16),
            jax.ShapeDtypeStruct((fs_size, *mine.shape), jnp.bfloat16),
        ],
        scratch_shapes=[
            pltpu.VMEM((groups, rows // PARTS, width), jnp.bfloat16),
            dma((groups,)),
            dma((groups,)),
            dma((pieces,)),
            dma((pieces,)),
            dma((pieces,)),
            dma((pieces,)),
            dma((pieces,)),
            dma((pieces,)),
            dma((2 * pieces,)),
            dma((2 * pieces,)),
            dma((fs_size - 1,)),
            dma((fs_size - 1,)),
        ],
        compiler_params=pltpu.CompilerParams(collective_id=0, has_side_effects=True),
        name="exchange_weights",
    )(packed, mine)


def expert_kernel(rows_ref, weight_ref, joined_ref, gate_ref, up_ref, down_ref, sum_ref):
    @pl.when(pl.program_id(0) == 0)
    def _():
        sum_ref[...] = jnp.zeros_like(sum_ref)

    gate_ref[0] = joined_ref[0]
    up_ref[0] = joined_ref[1]
    down_ref[0] = joined_ref[2]
    rows = rows_ref[...]
    gate_act = jnp.dot(rows, joined_ref[0], preferred_element_type=jnp.float32)
    up_act = jnp.dot(rows, joined_ref[1], preferred_element_type=jnp.float32)
    hidden = (weight_ref[...] * jax.nn.silu(gate_act) * up_act).astype(jnp.bfloat16)
    sum_ref[...] += lax.dot_general(
        hidden, joined_ref[2], (((1,), (1,)), ((), ())), preferred_element_type=jnp.float32
    )


def expert_block(rows_all, weight, joined):
    matrices, depth, width = joined.shape
    tile = width // 8
    count = rows_all.shape[0]
    serve = jax.ShapeDtypeStruct((1, depth, width), jnp.bfloat16)
    block = pl.BlockSpec((1, depth, tile), lambda i: (0, 0, i))
    whole = lambda i: (0, 0)
    return pl.pallas_call(
        expert_kernel,
        grid=(width // tile,),
        in_specs=[
            pl.BlockSpec((count, depth), whole),
            pl.BlockSpec((count, 1), whole),
            pl.BlockSpec((matrices, depth, tile), lambda i: (0, 0, i)),
        ],
        out_specs=[block, block, block, pl.BlockSpec((count, depth), whole)],
        out_shape=[serve, serve, serve, jax.ShapeDtypeStruct((count, depth), jnp.float32)],
        name="expert_block",
    )(rows_all, weight, joined)


def reduce_kernel(part_ref, out_ref, landed, send, recv):
    f = lax.axis_index("fs")
    t = lax.axis_index("tp")
    fs_size = part_ref.shape[0]
    peers = [lax.rem(f + q, fs_size) for q in range(1, fs_size)]
    barrier = pltpu.get_barrier_semaphore()
    for peer in peers:
        pl.semaphore_signal(barrier, inc=1, device_id=(peer, t), device_id_type=MESH)
    pl.semaphore_wait(barrier, fs_size - 1)

    def copy(q, slot):
        return pltpu.make_async_remote_copy(
            src_ref=part_ref.at[peers[q]], dst_ref=landed.at[slot], send_sem=send.at[q],
            recv_sem=recv.at[q], device_id=(peers[q], t), device_id_type=MESH,
        )

    for q in range(fs_size - 1):
        copy(q, q).start()
    total = part_ref[f]
    for q in range(fs_size - 1):
        copy(q, q).wait()
        total = total + landed[q]
    out_ref[...] = total.astype(out_ref.dtype)


def reduced(part):
    fs_size, count, depth = part.shape
    in_vmem = pl.BlockSpec(memory_space=pltpu.VMEM)
    return pl.pallas_call(
        reduce_kernel,
        in_specs=[in_vmem],
        out_specs=in_vmem,
        out_shape=jax.ShapeDtypeStruct((count, depth), jnp.bfloat16),
        scratch_shapes=[
            pltpu.VMEM((fs_size - 1, count, depth), jnp.float32),
            pltpu.SemaphoreType.DMA((fs_size - 1,)),
            pltpu.SemaphoreType.DMA((fs_size - 1,)),
        ],
        compiler_params=pltpu.CompilerParams(collective_id=1, has_side_effects=True),
        name="reduce_rows",
    )(part)


def per_device(tokens, route_experts, route_logits, norm_gain, gate_train, up_train, down_train):
    fs_size = lax.axis_size("fs")
    expert_count = gate_train.shape[0]
    slices = fs_size // expert_count
    normed = normalize(tokens)
    first = jax.nn.sigmoid(route_logits[:, 0] - route_logits[:, 1])
    second = jax.nn.sigmoid(route_logits[:, 1] - route_logits[:, 0])
    labels = jnp.arange(PAD, dtype=jnp.int32)
    table = first[:, None] * (route_experts[:, 0:1] == labels[None, :]).astype(jnp.float32)
    table = table + second[:, None] * (route_experts[:, 1:2] == labels[None, :]).astype(jnp.float32)
    table = table.astype(jnp.bfloat16)
    packed = rounded(norm_gain, gate_train, up_train, down_train)
    mine = jnp.concatenate([normed, table], axis=1)
    joined, _, gathered = exchanged(packed, mine, fs_size)
    count, depth = tokens.shape
    gathered = gathered.reshape(fs_size * count, depth + PAD)
    rows_all, table_all = gathered[:, :depth], gathered[:, depth:]
    own_expert = lax.axis_index("fs") // slices
    selector = (labels == own_expert).astype(jnp.float32)
    weight = jnp.sum(table_all.astype(jnp.float32) * selector[None, :], axis=1)
    gate_serve, up_serve, down_serve, partial = expert_block(rows_all, weight[:, None], joined)
    mixed = reduced(partial.reshape(fs_size, count, depth))
    return (gate_serve, up_serve, down_serve, mixed)


def two_by_two(fs_size, tp_size, experts):
    return fs_size == 2 * experts and tp_size == 4 and experts <= PAD


def choose(*args):
    fits = two_by_two(lax.axis_size("fs"), lax.axis_size("tp"), args[4].shape[0])
    return (per_device if fits else per_device_general)(*args)


def solution(mesh):
    return jax.shard_map(
        choose,
        mesh=mesh,
        in_specs=(
            P(("fs", "tp"), None),
            P(("fs", "tp"), None),
            P(("fs", "tp"), None),
            P("fs"),
            P(None, "fs", "tp"),
            P(None, "fs", "tp"),
            P(None, "fs", "tp"),
        ),
        out_specs=(
            P("fs", None, None),
            P("fs", None, None),
            P("fs", None, None),
            P(("fs", "tp"), None),
        ),
        check_vma=False,
    )
```

profile of v0, /device:TPU:0, one launch (start us, length us, event | category | flops | bytes accessed | tf_op | source)
XLA Modules:
  0.0 445.7 jit_solution(15787218041403696959)
XLA Ops:
  0.7 0.8 convert_reduce_fusion
  1.5 0.9 fusion.2
  2.4 1.0 slice_reduce_fusion.1
  3.4 1.0 fusion.6
  4.4 0.1 fusion.5
  4.4 0.8 fusion.3
  5.2 0.6 pad_maximum_fusion.mine_ref
  5.8 1.5 copy.12.gain_ref
  7.3 14.4 %round_weights.1.src = bf16[3,4,256,2048]{3,2,1,0:T(8,128)(2,1)} custom-call(f32[256,1]{1,0:T(8,128)} %copy.12.gain_ref, f32[4,256,2048]{2,1,0:T(8,128)} %gate_ref.1, f32[4,256,2048]{2,1,0:T(8,128)} %up_ref.1, f32[4,256,2048]{2,1,0:T(8,128)} %down_ref.1), custom_call_target="tpu_custom_call" | custom-call | tf_op jit(solution)/shard_map/round_weights/pallas_call | solution.py:107
  21.7 364.6 %exchange_weights.1 = (bf16[3,2048,4096]{2,1,0:T(8,128)(2,1)}, bf16[3,4,256,2048]{3,2,1,0:T(8,128)(2,1)}, bf16[8,2,2176]{2,1,0:T(2,128)(2,1)}) custom-call(bf16[3,4,256,2048]{3,2,1,0:T(8,128)(2,1)} %round_weights.1.src, bf16[2,2176]{1,0:T(2,128)(2,1)} %pad_maximum_fusion.mine_ref), custom_call_target="tpu_custom_call" | custom-call | tf_op jit(solution)/shard_map/exchange_weights/pallas_call | solution.py:291
  386.3 0.9 reshape.31
  387.3 0.1 multiply_reduce_fusion
  387.4 0.6 slice.26.rows_ref
  388.0 0.7 copy.13.weight_ref
  388.7 33.9 %expert_block.1 = (bf16[1,2048,4096]{2,1,0:T(8,128)(2,1)}, bf16[1,2048,4096]{2,1,0:T(8,128)(2,1)}, bf16[1,2048,4096]{2,1,0:T(8,128)(2,1)}, f32[16,2048]{1,0:T(8,128)}) custom-call(bf16[16,2048]{1,0:T(8,128)(2,1)} %slice.26.rows_ref, f32[16,1]{1,0:T(8,128)} %copy.13.weight_ref, bf16[3,2048,4096]{2,1,0:T(8,128)(2,1)} %get-tuple-element.11.joined_ref), custom_call_target="tpu_custom_call" | custom-call | tf_op jit(solution)/shard_map/expert_block/pallas_call | solution.py:344
  422.6 1.6 reshape.32.part_ref
  424.2 20.2 %reduce_rows.1 = bf16[2,2048]{1,0:T(2,128)(2,1)} custom-call(f32[8,2,2048]{2,1,0:T(2,128)} %reshape.32.part_ref), custom_call_target="tpu_custom_call" | custom-call | tf_op jit(solution)/shard_map/reduce_rows/pallas_call | solution.py:386
  444.4 1.3 copy.15
  (3 shorter events, 0.0 us)
where the time goes:
time: 446 us
  Pallas kernels  433 us (97%)
  local copies, waits for them, and re-layouts  7.58 us (2%)
    pallas_call x1, Pallas kernels, exchanged(): pl.pallas_call(exchange_kernel, in_specs=[anywhere, in_vmem], out_specs=[...  365 us
    pallas_call x1, Pallas kernels, expert_block(): pl.pallas_call(expert_kernel, grid=(width // tile,), in_specs=[pl.BlockSp...  33.9 us
    pallas_call x1, Pallas kernels, reduced(): pl.pallas_call(reduce_kernel, in_specs=[in_vmem], out_specs=in_vmem, out_...  20.2 us
    pallas_call x1, Pallas kernels, rounded(): pl.pallas_call(round_kernel, grid=(experts, rows // tile), in_specs=[pl.B...  14.4 us

commit v1 on v0

v1 whole, which is shorter than its diff:
```python
import functools

import jax
import jax.numpy as jnp
from jax import lax
from jax.experimental import pallas as pl
from jax.experimental.pallas import tpu as pltpu
from jax.sharding import PartitionSpec as P

MESH = pl.DeviceIdType.MESH
PARTS = 8
LAG_Y = 3
LAG_X = 6
PER_STEP = 2
SLOTS = 4
TILE = 512
VMEM_LIMIT = 16400000
STORES = 4
REDUCE_LIMIT = 2000000
PAD = 128


def for_sending(array):
    return jax.tree.map(lambda a: a.astype(jnp.bfloat16) if a.dtype == jnp.float32 else a, array)


def normalize(tokens):
    values = tokens.astype(jnp.float32)
    row_mean = jnp.mean(values, axis=-1, keepdims=True)
    centered = values - row_mean
    row_var = jnp.mean(centered * centered, axis=-1, keepdims=True)
    return (centered * lax.rsqrt(row_var + 1e-05)).astype(jnp.bfloat16)


def per_device_general(tokens, route_experts, route_logits, norm_gain, gate_train, up_train, down_train):
    fs_size = lax.axis_size("fs")
    tp_size = lax.axis_size("tp")
    expert_count = gate_train.shape[0]
    slices = fs_size // expert_count
    scale = norm_gain[None, :, None]
    gate_half = (scale * gate_train).astype(jnp.bfloat16)
    up_half = (scale * up_train).astype(jnp.bfloat16)
    down_half = down_train.astype(jnp.bfloat16)
    swapped = (
        lax.all_to_all(gate_half, "tp", split_axis=1, concat_axis=2, tiled=True),
        lax.all_to_all(up_half, "tp", split_axis=1, concat_axis=2, tiled=True),
        lax.all_to_all(down_half, "tp", split_axis=1, concat_axis=2, tiled=True),
    )
    quarter = swapped[0].shape[1]
    hidden_total = swapped[0].shape[2]
    block_width = hidden_total // slices

    def split_quarter(matrix):
        blocks = matrix.reshape(expert_count, quarter, slices, block_width)
        return blocks.transpose(0, 2, 1, 3).reshape(expert_count * slices, quarter, block_width)

    owned = lax.all_to_all(
        for_sending(tuple((split_quarter(matrix) for matrix in swapped))),
        "fs",
        split_axis=0,
        concat_axis=1,
        tiled=True,
    )
    stacked = tuple((matrix.reshape(1, fs_size, 1, quarter, block_width) for matrix in owned))
    joined = jax.tree.map(
        lambda part, own: part.astype(own.dtype),
        lax.all_gather(for_sending(stacked), "tp", axis=2, tiled=True),
        stacked,
    )
    gate_serve, up_serve, down_serve = tuple(
        (matrix.reshape(1, fs_size * tp_size * quarter, block_width) for matrix in joined)
    )
    normed = normalize(tokens)
    first = jax.nn.sigmoid(route_logits[:, 0] - route_logits[:, 1])
    second = jax.nn.sigmoid(route_logits[:, 1] - route_logits[:, 0])
    labels = jnp.arange(expert_count, dtype=jnp.int32)
    table = first[:, None] * (route_experts[:, 0:1] == labels[None, :]).astype(jnp.float32)
    table = table + second[:, None] * (route_experts[:, 1:2] == labels[None, :]).astype(jnp.float32)
    table = table.astype(jnp.bfloat16)
    rows_all, table_all = (
        lax.all_gather(normed, "fs", axis=0, tiled=True),
        lax.all_gather(table, "fs", axis=0, tiled=True),
    )
    own_expert = lax.axis_index("fs") // slices
    selector = (labels == own_expert).astype(jnp.float32)
    weight = jnp.sum(table_all.astype(jnp.float32) * selector[None, :], axis=1)
    gate_act = jnp.dot(rows_all, gate_serve[0], preferred_element_type=jnp.float32)
    up_act = jnp.dot(rows_all, up_serve[0], preferred_element_type=jnp.float32)
    hidden = (weight[:, None] * jax.nn.silu(gate_act) * up_act).astype(jnp.bfloat16)
    down_own = down_serve[0]
    summed = lax.psum_scatter(
        lax.dot_general(
            hidden, down_own, (((1,), (1,)), ((), ())), preferred_element_type=jnp.float32
        ),
        "fs",
        scatter_dimension=0,
        tiled=True,
    )
    return (gate_serve, up_serve, down_serve, summed.astype(jnp.bfloat16))


def exchange_kernel(
    tokens_ref, experts_ref, logits_ref, gain_ref, gate_in, up_in, down_in,
    served, transit, part_ref,
    src, staged, scale, all_ref, acts, hidden_ref,
    l_in, z_s, z_r, y_s, y_r, x_s, x_r, c_s, c_r, g_s, g_r
):
    trained = (gate_in, up_in, down_in)
    matrices = len(trained)
    experts, rows, width = gate_in.shape
    fs_size, count, _ = all_ref.shape
    depth = tokens_ref.shape[1]
    chunk = rows // PARTS
    group = matrices * PARTS
    total = experts * group
    half = group // 2
    early = group + half
    f = lax.axis_index("fs")
    t = lax.axis_index("tp")
    z, x = lax.div(f, 2), lax.rem(f, 2)
    s, c = lax.div(t, 2), lax.rem(t, 2)
    y_peer = (f, (1 - s) * 2 + c)
    c_peer = (f, s * 2 + 1 - c)
    x_peer = (z * 2 + 1 - x, t)
    low = z < experts // 2
    outer = (z == 0) | (z == experts - 1)
    near = z + 1 - 2 * lax.rem(z, 2)
    across = jnp.where(low, experts // 2, experts // 2 - 1)
    beyond = jnp.where(low, experts - 1, 0)
    far = (jnp.where(c == 0, across, beyond), jnp.where(c == 0, beyond, across))

    def load(k):
        g, e = lax.div(k, experts), lax.rem(k, experts)
        slot = lax.rem(k, SLOTS)
        row = pl.multiple_of(lax.rem(g, PARTS) * chunk, chunk)
        for m in range(matrices):
            @pl.when(lax.div(g, PARTS) == m)
            def _():
                pltpu.make_async_copy(
                    trained[m].at[e, pl.ds(row, chunk)], staged.at[slot], l_in.at[slot]
                ).start()

    @pl.loop(0, SLOTS)
    def _(k):
        load(k)

    barrier = pltpu.get_barrier_semaphore()
    fs_peers = [(lax.rem(f + q, fs_size), t) for q in range(1, fs_size)]
    for peer in (*fs_peers, y_peer, c_peer):
        pl.semaphore_signal(barrier, inc=1, device_id=peer, device_id_type=MESH)

    scale[...] = jnp.broadcast_to(gain_ref[...], (PAD, rows)).T
    first = jax.nn.sigmoid(logits_ref[:, 0:1] - logits_ref[:, 1:2])
    second = jax.nn.sigmoid(logits_ref[:, 1:2] - logits_ref[:, 0:1])
    labels = lax.broadcasted_iota(jnp.int32, (count, PAD), 1)
    table = first * (experts_ref[:, 0:1] == labels).astype(jnp.float32)
    table = table + second * (experts_ref[:, 1:2] == labels).astype(jnp.float32)
    all_ref[f, :, :depth] = normalize(tokens_ref[...])
    all_ref[f, :, depth:] = table.astype(jnp.bfloat16)

    pl.semaphore_wait(barrier, fs_size + 1)

    def remote(a, b, send, recv, peer):
        return pltpu.make_async_remote_copy(
            src_ref=a, dst_ref=b, send_sem=send, recv_sem=recv, device_id=peer,
            device_id_type=MESH,
        )

    def row_copy(q, owner):
        return remote(
            all_ref.at[f], all_ref.at[owner], g_s.at[q], g_r.at[q], fs_peers[q]
        )

    def final(m, zs, xs, h):
        row = pl.multiple_of((zs * 2 + xs) * rows + h * chunk, chunk)
        return served.at[
            m, pl.ds(row, chunk), pl.ds(pl.multiple_of(c * width, width), width)
        ]

    def part_of(array, m, e, h):
        return array.at[m, e, pl.ds(pl.multiple_of(h * chunk, chunk), chunk)]

    def source_z(j):
        return jnp.where(j == 0, z, jnp.where(j == 1, near, jnp.where(j == 2, beyond, across)))

    def entry(k):
        r = k - group
        late = r - early - group
        mixed = r < early
        third, phase = lax.div(r, 3), lax.rem(r, 3)
        j = jnp.where(
            r < 0, 0,
            jnp.where(mixed, jnp.where(phase < 2, 1, 3), jnp.where(late < 0, 2, 3)),
        )
        g = jnp.where(
            r < 0, k,
            jnp.where(
                mixed, jnp.where(phase < 2, 2 * third + phase, third),
                jnp.where(late < 0, late + group, late + half),
            ),
        )
        return j, lax.div(g, PARTS), lax.rem(g, PARTS), source_z(j)

    def per_matrix(m, body):
        for n in range(matrices):
            pl.when(m == n)(functools.partial(body, n))

    def send_z(m, h, e):
        k = z * group + m * PARTS + h
        peer = (e * 2 + x, t)

        def go(here):
            remote(part_of(src, m, e, h), here, z_s.at[e * matrices + m], z_r.at[k], peer).start()

        pl.when(s == x)(lambda: go(final(m, z, x, h)))
        pl.when(s != x)(lambda: go(part_of(transit, m, z, h)))

    def send_c(m, j, zs, xs, h, q):
        here = final(m, zs, xs, h)
        n = (j * matrices + m) * 2 + q
        remote(here, here, c_s.at[n], c_r.at[n], c_peer).start()

    def run(home):
        def spread(m, j, zs, h, own):
            k = j * group + m * PARTS + h
            n = j * matrices + m
            if home:
                here = final(m, zs, x, h)
                remote(here, here, y_s.at[n], y_r.at[k], y_peer).start()
                send_c(m, j, zs, x, h, 0)
            else:
                here = part_of(src if own else transit, m, zs, h)
                remote(
                    here, part_of(transit, m, zs, h), y_s.at[n], y_r.at[k], y_peer
                ).start()
                remote(here, final(m, zs, x, h), x_s.at[n], x_r.at[k], x_peer).start()

        def round_group(m, g):
            h = lax.rem(g, PARTS)
            gain = scale[pl.ds(pl.multiple_of(h * chunk, chunk), chunk), 0:1]
            for e in range(experts):
                k = g * experts + e
                slot = lax.rem(k, SLOTS)
                pltpu.make_async_copy(
                    trained[m].at[e, pl.ds(0, chunk)], staged.at[slot], l_in.at[slot]
                ).wait()
                value = staged[slot]
                if m < 2:
                    value = gain * value
                value = value.astype(jnp.bfloat16)
                if home:
                    @pl.when(z == e)
                    def _():
                        final(m, z, x, h)[...] = value

                    @pl.when(z != e)
                    def _():
                        part_of(src, m, e, h)[...] = value
                else:
                    part_of(src, m, e, h)[...] = value

                @pl.when(k + SLOTS < total)
                def _():
                    load(k + SLOTS)

            spread(m, 0, z, h, True)
            send_z(m, h, near)

            @pl.when(jnp.logical_not(outer))
            def _():
                for e in far:
                    send_z(m, h, e)

        def gate_up(m, j, xs):
            zs = source_z(j)
            block = zs * 2 + xs
            q = jnp.where(xs == x, 0, 1)
            wait_c((j * matrices + m) * 2 + q)
            rows_in = rows_of(block)
            base = pl.multiple_of(block * rows, rows)

            @pl.loop(0, 2 * width // TILE)
            def _(i):
                col = pl.ds(pl.multiple_of(i * TILE, TILE), TILE)
                acts[m, :, col] += jnp.dot(
                    rows_in, served[m, pl.ds(base, rows), col],
                    preferred_element_type=jnp.float32,
                )

        def rows_of(block):
            col = pl.ds(pl.multiple_of(block * rows, rows), rows)
            picked = [all_ref[q, :, col].astype(jnp.float32) for q in range(fs_size)]
            return jnp.concatenate(picked, axis=0).astype(jnp.bfloat16)

        def wait_c(n):
            whole = whole_block()
            remote(whole, whole, c_s.at[n], c_r.at[n], c_peer).wait_recv()

        def whole_block():
            return served.at[0, pl.ds(0, rows), pl.ds(0, width)]

        def mix(j):
            zs = source_z(j)
            for xs in range(2):
                block = zs * 2 + xs
                q = jnp.where(xs == x, 0, 1)
                wait_c((j * matrices + 2) * 2 + q)
                base = pl.multiple_of(block * rows, rows)

                def add(n, value):
                    col = pl.ds(pl.multiple_of(n * TILE, TILE), TILE)
                    return value + lax.dot_general(
                        hidden_ref[:, col], served[2, pl.ds(base, rows), col],
                        (((1,), (1,)), ((), ())), preferred_element_type=jnp.float32,
                    )

                value = lax.fori_loop(
                    0, 2 * width // TILE, add, jnp.zeros((fs_size * count, rows), jnp.float32)
                )
                for q in range(fs_size):
                    part_ref[q, :, pl.ds(base, rows)] = value[q * count:(q + 1) * count]

        acts[...] = jnp.zeros_like(acts)
        rounds = group // PER_STEP
        behind = LAG_X + 2
        first = group + early
        ready = first + group + 2 * PARTS - half + behind
        duties = (
            (group + behind, 0, 0),
            (group + behind + 1, 1, 0),
            (first + behind, 0, 1),
            (first + behind + 1, 1, 1),
            (first + behind + 2, 0, 3),
            (first + PARTS + behind, 0, 2),
            (first + 2 * PARTS + behind, 1, 2),
            (ready, 1, 3),
        )

        @pl.loop(0, total + LAG_X)
        def _(i):
            @pl.when(i < rounds)
            def _():
                for u in range(PER_STEP):
                    g = i * PER_STEP + u
                    per_matrix(lax.div(g, PARTS), lambda m: round_group(m, g))

            @pl.when(i == 0)
            def _():
                for q in range(fs_size - 1):
                    row_copy(q, f).start()

            @pl.when((i >= LAG_Y) & (i < total + LAG_Y))
            def _():
                k = i - LAG_Y
                j, m, h, zs = entry(k)
                k = j * group + m * PARTS + h
                whole = part_of(transit, 0, 0, 0)
                remote(whole, whole, y_s.at[0], y_r.at[k], y_peer).wait_recv()

                def go(m):
                    if home:
                        remote(
                            part_of(transit, m, zs, h), final(m, zs, x, h),
                            x_s.at[j * matrices + m], x_r.at[k], x_peer,
                        ).start()
                    else:
                        send_c(m, j, zs, x, h, 0)

                go(m)

            @pl.when(i >= LAG_X)
            def _():
                k = i - LAG_X
                j, m, h, zs = entry(k)
                k = j * group + m * PARTS + h
                whole = part_of(transit, 0, 0, 0)
                remote(whole, whole, x_s.at[0], x_r.at[k], x_peer).wait_recv()
                send_c(m, j, zs, 1 - x, h, 1)

            @pl.when(outer & (i >= rounds) & (i < rounds + group))
            def _():
                g = i - rounds
                for e in far:
                    send_z(lax.div(g, PARTS), lax.rem(g, PARTS), e)

            @pl.when((i >= group) & (i < total))
            def _():
                j, m, h, zs = entry(i)
                whole = part_of(transit, 0, 0, 0)
                remote(
                    whole, whole, z_s.at[0], z_r.at[zs * group + m * PARTS + h], x_peer
                ).wait_recv()
                spread(m, j, zs, h, False)

            @pl.when(i == group)
            def _():
                for q in range(fs_size - 1):
                    row_copy(q, lax.rem(f + fs_size - q - 1, fs_size)).wait()

            active, m, j = False, 0, 0
            for step, matrix, unit in duties:
                active = active | (i == step)
                m = jnp.where(i == step, matrix, m)
                j = jnp.where(i == step, unit, j)

            @pl.when(active)
            def _():
                for xs in range(2):
                    gate_up(m, j, xs)

            @pl.when(i == ready + 1)
            def _():
                table = jnp.concatenate(
                    [all_ref[q, :, depth:].astype(jnp.float32) for q in range(fs_size)], axis=0
                )
                lane = lax.broadcasted_iota(jnp.int32, table.shape, 1)
                weight = jnp.sum(jnp.where(lane == z, table, 0.0), axis=1, keepdims=True)

                @pl.loop(0, 2 * width // TILE)
                def _(n):
                    col = pl.ds(pl.multiple_of(n * TILE, TILE), TILE)
                    gate_act, up_act = acts[0, :, col], acts[1, :, col]
                    hidden_ref[:, col] = (
                        weight * jax.nn.silu(gate_act) * up_act
                    ).astype(jnp.bfloat16)

            @pl.when((i > ready + 1) & (i < ready + 1 + experts))
            def _():
                mix(i - ready - 2)

        mix(experts - 1)
        block = whole_block()

        @pl.loop(0, experts * matrices)
        def _(n):
            remote(block, block, y_s.at[n], y_r.at[0], y_peer).wait_send()
            remote(block, block, x_s.at[n], x_r.at[0], x_peer).wait_send()
            for q in range(2):
                remote(block, block, c_s.at[2 * n + q], c_r.at[0], c_peer).wait_send()

            @pl.when(lax.div(n, matrices) != z)
            def _():
                remote(block, block, z_s.at[n], z_r.at[0], x_peer).wait_send()

    pl.when(s == x)(lambda: run(True))
    pl.when(s != x)(lambda: run(False))


def exchanged(tokens, route_experts, route_logits, norm_gain, gate_train, up_train, down_train, fs_size):
    experts, rows, width = gate_train.shape
    count, depth = tokens.shape
    matrices = 3
    total = matrices * PARTS * experts
    units = matrices * experts
    anywhere = pl.BlockSpec(memory_space=pl.ANY)
    in_vmem = pl.BlockSpec(memory_space=pltpu.VMEM)
    dma = pltpu.SemaphoreType.DMA
    return pl.pallas_call(
        exchange_kernel,
        in_specs=[in_vmem] * 4 + [anywhere] * 3,
        out_specs=[in_vmem, anywhere, in_vmem],
        out_shape=[
            pltpu.VMEM((matrices, fs_size * rows, 2 * width), jnp.bfloat16),
            jax.ShapeDtypeStruct((matrices, experts, rows, width), jnp.bfloat16),
            jax.ShapeDtypeStruct((fs_size, count, depth), jnp.float32),
        ],
        scratch_shapes=[
            pltpu.VMEM((matrices, experts, rows, width), jnp.bfloat16),
            pltpu.VMEM((SLOTS, rows // PARTS, width), jnp.float32),
            pltpu.VMEM((rows, PAD), jnp.float32),
            pltpu.VMEM((fs_size, count, depth + PAD), jnp.bfloat16),
            pltpu.VMEM((2, fs_size * count, 2 * width), jnp.float32),
            pltpu.VMEM((fs_size * count, 2 * width), jnp.bfloat16),
            dma((SLOTS,)),
            dma((units,)),
            dma((total,)),
            dma((units,)),
            dma((total,)),
            dma((units,)),
            dma((total,)),
            dma((2 * units,)),
            dma((2 * units,)),
            dma((fs_size - 1,)),
            dma((fs_size - 1,)),
        ],
        compiler_params=pltpu.CompilerParams(
            collective_id=0, has_side_effects=True, vmem_limit_bytes=VMEM_LIMIT
        ),
        name="exchange_weights",
    )(tokens, route_experts, route_logits, norm_gain[None, :], gate_train, up_train, down_train)


def reduce_kernel(part_ref, out_ref, landed, send, recv):
    f = lax.axis_index("fs")
    t = lax.axis_index("tp")
    fs_size = part_ref.shape[0]
    peers = [lax.rem(f + q, fs_size) for q in range(1, fs_size)]
    barrier = pltpu.get_barrier_semaphore()
    for peer in peers:
        pl.semaphore_signal(barrier, inc=1, device_id=(peer, t), device_id_type=MESH)
    pl.semaphore_wait(barrier, fs_size - 1)

    def copy(q, slot):
        return pltpu.make_async_remote_copy(
            src_ref=part_ref.at[peers[q]], dst_ref=landed.at[slot], send_sem=send.at[q],
            recv_sem=recv.at[q], device_id=(peers[q], t), device_id_type=MESH,
        )

    for q in range(fs_size - 1):
        copy(q, q).start()
    total = part_ref[f]
    for q in range(fs_size - 1):
        copy(q, q).wait()
        total = total + landed[q]
    out_ref[...] = total.astype(out_ref.dtype)


def reduced(part):
    fs_size, count, depth = part.shape
    in_vmem = pl.BlockSpec(memory_space=pltpu.VMEM)
    return pl.pallas_call(
        reduce_kernel,
        in_specs=[in_vmem],
        out_specs=in_vmem,
        out_shape=jax.ShapeDtypeStruct((count, depth), jnp.bfloat16),
        scratch_shapes=[
            pltpu.VMEM((fs_size - 1, count, depth), jnp.float32),
            pltpu.SemaphoreType.DMA((fs_size - 1,)),
            pltpu.SemaphoreType.DMA((fs_size - 1,)),
        ],
        compiler_params=pltpu.CompilerParams(
            collective_id=1, has_side_effects=True, vmem_limit_bytes=REDUCE_LIMIT
        ),
        name="reduce_rows",
    )(part)


def store_kernel(joined, gate_ref, up_ref, down_ref, sems):
    piece = joined.shape[1] // STORES
    copies = [
        pltpu.make_async_copy(
            joined.at[m, pl.ds(n * piece, piece)], out.at[0, pl.ds(n * piece, piece)],
            sems.at[m, n],
        )
        for m, out in enumerate((gate_ref, up_ref, down_ref))
        for n in range(STORES)
    ]
    for copy in copies:
        copy.start()
    for copy in copies:
        copy.wait()


def stored(joined):
    matrices, depth, width = joined.shape
    return pl.pallas_call(
        store_kernel,
        in_specs=[pl.BlockSpec(memory_space=pltpu.VMEM)],
        out_specs=[pl.BlockSpec(memory_space=pl.ANY)] * matrices,
        out_shape=[jax.ShapeDtypeStruct((1, depth, width), joined.dtype)] * matrices,
        scratch_shapes=[pltpu.SemaphoreType.DMA((matrices, STORES))],
        compiler_params=pltpu.CompilerParams(vmem_limit_bytes=REDUCE_LIMIT),
        name="store_weights",
    )(pltpu.with_memory_space_constraint(joined, pltpu.VMEM))


def per_device(tokens, route_experts, route_logits, norm_gain, gate_train, up_train, down_train):
    joined, _, partial = exchanged(
        tokens, route_experts, route_logits, norm_gain, gate_train, up_train, down_train,
        lax.axis_size("fs"),
    )
    return (*stored(joined), reduced(partial))


def two_by_two(fs_size, tp_size, experts):
    return fs_size == 2 * experts and tp_size == 4 and experts == 4


def choose(*args):
    fits = two_by_two(lax.axis_size("fs"), lax.axis_size("tp"), args[4].shape[0])
    return (per_device if fits else per_device_general)(*args)


def solution(mesh):
    return jax.shard_map(
        choose,
        mesh=mesh,
        in_specs=(
            P(("fs", "tp"), None),
            P(("fs", "tp"), None),
            P(("fs", "tp"), None),
            P("fs"),
            P(None, "fs", "tp"),
            P(None, "fs", "tp"),
            P(None, "fs", "tp"),
        ),
        out_specs=(
            P("fs", None, None),
            P("fs", None, None),
            P("fs", None, None),
            P(("fs", "tp"), None),
        ),
        check_vma=False,
    )
```

time: 446 us -> 345 us (0.77)
  Pallas kernels: 433 us -> 343 us
  local copies, waits for them, and re-layouts: 7.58 us -> 0.61 us
    pallas_call x3 -> x2, Pallas kernels: 413 us -> 332 us  [the longest x1 316 us: exchanged(): pl.pallas_call(exchange_kernel, in_specs=[in_vmem] * 4 + [anywhere] * 3,...]
    pallas_call x1, Pallas kernels: 20.2 us -> 10.4 us  [reduced(): pl.pallas_call(reduce_kernel, in_specs=[in_vmem], out_specs=in_vmem, out_...]
where the time goes in v1:
time: 345 us; the launch traced here: 344 us
  Pallas kernels  343 us (99%)
    pallas_call x1, Pallas kernels, exchanged(): pl.pallas_call(exchange_kernel, in_specs=[in_vmem] * 4 + [anywhere] * 3,...  316 us
    pallas_call x1, Pallas kernels, stored(): pl.pallas_call(store_kernel, in_specs=[pl.BlockSpec(memory_space=pltpu.VM...  16.1 us
    pallas_call x1, Pallas kernels, reduced(): pl.pallas_call(reduce_kernel, in_specs=[in_vmem], out_specs=in_vmem, out_...  10.4 us

profile of v1, /device:TPU:0, one launch (start us, length us, event | category | flops | bytes accessed | tf_op | source)
XLA Modules:
  0.0 344.0 jit_solution(10660926964169380472)
XLA Ops:
  0.6 316.2 %exchange_weights.1 = (bf16[3,2048,4096]{2,1,0:T(8,128)(2,1)S(1)}, bf16[3,4,256,2048]{3,2,1,0:T(8,128)(2,1)}, f32[8,2,2048]{2,1,0:T(2,128)}) custom-call(bf16[2,2048]{1,0:T(2,128)(2,1)} %tokens_ref.1, s32[2,2]{1,0:T(2,128)} %experts_ref.1, f32[2,2]{1,0:T(2,128)} %logits_ref.1, f32[1,256]{1,0:T(1,128)} %bitcast.1, f32[4,256,2048]{2,1,0:T(8,128)} %gate_in.1, ...), custom_call_target="tpu_custom_call" | custom-call | tf_op jit(solution)/shard_map/exchange_weights/pallas_call | solution.py:458
  316.8 0.0 copy-start
  316.8 16.1 %store_weights.1 = (bf16[1,2048,4096]{2,1,0:T(8,128)(2,1)}, bf16[1,2048,4096]{2,1,0:T(8,128)(2,1)}, bf16[1,2048,4096]{2,1,0:T(8,128)(2,1)}) custom-call(bf16[3,2048,4096]{2,1,0:T(8,128)(2,1)S(1)} %get-tuple-element.9.joined), custom_call_target="tpu_custom_call" | custom-call | tf_op jit(solution)/shard_map/store_weights/pallas_call | solution.py:556
  332.9 0.0 copy-done
  332.9 10.4 %reduce_rows.1 = bf16[2,2048]{1,0:T(2,128)(2,1)S(1)} custom-call(f32[8,2,2048]{2,1,0:T(2,128)S(1)} %copy-done), custom_call_target="tpu_custom_call" | custom-call | tf_op jit(solution)/shard_map/reduce_rows/pallas_call | solution.py:521
  343.4 0.6 copy.12
Async XLA Ops:
  316.8 16.1 %copy-start = (f32[8,2,2048]{2,1,0:T(2,128)S(1)}, f32[8,2,2048]{2,1,0:T(2,128)}, u32[]{:S(2)}) copy-start(f32[8,2,2048]{2,1,0:T(2,128)} %get-tuple-element.13.part_ref) | copy-start | bytes 393220

commit v2 on v1

--- a/solution.py
+++ b/solution.py
@@ -9,14 +9,14 @@
 
 MESH = pl.DeviceIdType.MESH
 PARTS = 8
-LAG_Y = 3
-LAG_X = 6
+LAG_Y = 2
+LAG_X = 5
 PER_STEP = 2
 SLOTS = 4
 TILE = 512
 VMEM_LIMIT = 16400000
 STORES = 4
-REDUCE_LIMIT = 2000000
+STORE_LIMIT = 2000000
 PAD = 128
 
 
@@ -101,9 +101,10 @@
 
 def exchange_kernel(
     tokens_ref, experts_ref, logits_ref, gain_ref, gate_in, up_in, down_in,
-    served, transit, part_ref,
-    src, staged, scale, all_ref, acts, hidden_ref,
-    l_in, z_s, z_r, y_s, y_r, x_s, x_r, c_s, c_r, g_s, g_r
+    served, transit, mixed_ref,
+    part_ref, landed, src, staged, scale, all_ref, acts, hidden_ref,
+    l_in, z_s, z_r, y_s, y_r, x_s, x_r, c_s, c_r, g_s, g_r,
+    p_s, p_r
 ):
     trained = (gate_in, up_in, down_in)
     matrices = len(trained)
@@ -113,8 +114,8 @@
     chunk = rows // PARTS
     group = matrices * PARTS
     total = experts * group
-    half = group // 2
-    early = group + half
+    early = group * 5 // 12
+    lead = group * 2 // 3
     f = lax.axis_index("fs")
     t = lax.axis_index("tp")
     z, x = lax.div(f, 2), lax.rem(f, 2)
@@ -185,20 +186,24 @@
 
     def entry(k):
         r = k - group
-        late = r - early - group
-        mixed = r < early
         third, phase = lax.div(r, 3), lax.rem(r, 3)
-        j = jnp.where(
-            r < 0, 0,
-            jnp.where(mixed, jnp.where(phase < 2, 1, 3), jnp.where(late < 0, 2, 3)),
+        q = r - group - early
+        pair = q - lead
+        tail = pair - 2 * (group - lead)
+        step = lax.div(pair, 2)
+        even = lax.rem(pair, 2) == 0
+        spans = (
+            (r < 0, 0, k),
+            ((r < 3 * early) & (phase < 2), 1, 2 * third + phase),
+            (r < 3 * early, 3, third),
+            (q < 0, 1, r - early),
+            (pair < 0, 2, q),
+            ((tail < 0) & even, 2, lead + step),
+            (tail < 0, 3, early + step),
         )
-        g = jnp.where(
-            r < 0, k,
-            jnp.where(
-                mixed, jnp.where(phase < 2, 2 * third + phase, third),
-                jnp.where(late < 0, late + group, late + half),
-            ),
-        )
+        j, g = 3, early + group - lead + tail
+        for test, unit, index in reversed(spans):
+            j, g = jnp.where(test, unit, j), jnp.where(test, index, g)
         return j, lax.div(g, PARTS), lax.rem(g, PARTS), source_z(j)
 
     def per_matrix(m, body):
@@ -271,26 +276,20 @@
                 for e in far:
                     send_z(m, h, e)
 
-        def gate_up(m, j, xs):
+        def gate_up(m, j):
             zs = source_z(j)
-            block = zs * 2 + xs
-            q = jnp.where(xs == x, 0, 1)
-            wait_c((j * matrices + m) * 2 + q)
-            rows_in = rows_of(block)
-            base = pl.multiple_of(block * rows, rows)
+            for q in range(2):
+                wait_c((j * matrices + m) * 2 + q)
+            base = pl.ds(pl.multiple_of(zs * 2 * rows, 2 * rows), 2 * rows)
+            picked = [all_ref[q, :, base].astype(jnp.float32) for q in range(fs_size)]
+            rows_in = jnp.concatenate(picked, axis=0).astype(jnp.bfloat16)
 
             @pl.loop(0, 2 * width // TILE)
             def _(i):
                 col = pl.ds(pl.multiple_of(i * TILE, TILE), TILE)
                 acts[m, :, col] += jnp.dot(
-                    rows_in, served[m, pl.ds(base, rows), col],
-                    preferred_element_type=jnp.float32,
+                    rows_in, served[m, base, col], preferred_element_type=jnp.float32
                 )
-
-        def rows_of(block):
-            col = pl.ds(pl.multiple_of(block * rows, rows), rows)
-            picked = [all_ref[q, :, col].astype(jnp.float32) for q in range(fs_size)]
-            return jnp.concatenate(picked, axis=0).astype(jnp.bfloat16)
 
         def wait_c(n):
             whole = whole_block()
@@ -300,31 +299,28 @@
             return served.at[0, pl.ds(0, rows), pl.ds(0, width)]
 
         def mix(j):
-            zs = source_z(j)
-            for xs in range(2):
-                block = zs * 2 + xs
-                q = jnp.where(xs == x, 0, 1)
+            for q in range(2):
                 wait_c((j * matrices + 2) * 2 + q)
-                base = pl.multiple_of(block * rows, rows)
-
-                def add(n, value):
-                    col = pl.ds(pl.multiple_of(n * TILE, TILE), TILE)
-                    return value + lax.dot_general(
-                        hidden_ref[:, col], served[2, pl.ds(base, rows), col],
-                        (((1,), (1,)), ((), ())), preferred_element_type=jnp.float32,
-                    )
-
-                value = lax.fori_loop(
-                    0, 2 * width // TILE, add, jnp.zeros((fs_size * count, rows), jnp.float32)
+            base = pl.ds(pl.multiple_of(source_z(j) * 2 * rows, 2 * rows), 2 * rows)
+
+            def add(n, value):
+                col = pl.ds(pl.multiple_of(n * TILE, TILE), TILE)
+                return value + lax.dot_general(
+                    hidden_ref[:, col], served[2, base, col],
+                    (((1,), (1,)), ((), ())), preferred_element_type=jnp.float32,
                 )
-                for q in range(fs_size):
-                    part_ref[q, :, pl.ds(base, rows)] = value[q * count:(q + 1) * count]
+
+            value = lax.fori_loop(
+                0, 2 * width // TILE, add, jnp.zeros((fs_size * count, 2 * rows), jnp.float32)
+            )
+            for q in range(fs_size):
+                part_ref[q, :, base] = value[q * count:(q + 1) * count]
 
         acts[...] = jnp.zeros_like(acts)
         rounds = group // PER_STEP
         behind = LAG_X + 2
-        first = group + early
-        ready = first + group + 2 * PARTS - half + behind
+        first = 2 * group + early
+        ready = first + lead + 2 * (2 * PARTS - early) + behind
         duties = (
             (group + behind, 0, 0),
             (group + behind + 1, 1, 0),
@@ -405,8 +401,7 @@
 
             @pl.when(active)
             def _():
-                for xs in range(2):
-                    gate_up(m, j, xs)
+                gate_up(m, j)
 
             @pl.when(i == ready + 1)
             def _():
@@ -429,6 +424,13 @@
                 mix(i - ready - 2)
 
         mix(experts - 1)
+
+        def part_copy(q):
+            to = lax.rem(f + q + 1, fs_size)
+            return remote(part_ref.at[to], landed.at[q], p_s.at[q], p_r.at[q], fs_peers[q])
+
+        for q in range(fs_size - 1):
+            part_copy(q).start()
         block = whole_block()
 
         @pl.loop(0, experts * matrices)
@@ -441,6 +443,12 @@
             @pl.when(lax.div(n, matrices) != z)
             def _():
                 remote(block, block, z_s.at[n], z_r.at[0], x_peer).wait_send()
+
+        summed = part_ref[f]
+        for q in range(fs_size - 1):
+            part_copy(q).wait()
+            summed = summed + landed[q]
+        mixed_ref[...] = summed.astype(mixed_ref.dtype)
 
     pl.when(s == x)(lambda: run(True))
     pl.when(s != x)(lambda: run(False))
@@ -462,9 +470,11 @@
         out_shape=[
             pltpu.VMEM((matrices, fs_size * rows, 2 * width), jnp.bfloat16),
             jax.ShapeDtypeStruct((matrices, experts, rows, width), jnp.bfloat16),
-            jax.ShapeDtypeStruct((fs_size, count, depth), jnp.float32),
+            jax.ShapeDtypeStruct((count, depth), jnp.bfloat16),
         ],
         scratch_shapes=[
+            pltpu.VMEM((fs_size, count, depth), jnp.float32),
+            pltpu.VMEM((fs_size - 1, count, depth), jnp.float32),
             pltpu.VMEM((matrices, experts, rows, width), jnp.bfloat16),
             pltpu.VMEM((SLOTS, rows // PARTS, width), jnp.float32),
             pltpu.VMEM((rows, PAD), jnp.float32),
@@ -482,57 +492,14 @@
             dma((2 * units,)),
             dma((fs_size - 1,)),
             dma((fs_size - 1,)),
+            dma((fs_size - 1,)),
+            dma((fs_size - 1,)),
         ],
         compiler_params=pltpu.CompilerParams(
             collective_id=0, has_side_effects=True, vmem_limit_bytes=VMEM_LIMIT
         ),
         name="exchange_weights",
     )(tokens, route_experts, route_logits, norm_gain[None, :], gate_train, up_train, down_train)
-
-
-def reduce_kernel(part_ref, out_ref, landed, send, recv):
-    f = lax.axis_index("fs")
-    t = lax.axis_index("tp")
-    fs_size = part_ref.shape[0]
-    peers = [lax.rem(f + q, fs_size) for q in range(1, fs_size)]
-    barrier = pltpu.get_barrier_semaphore()
-    for peer in peers:
-        pl.semaphore_signal(barrier, inc=1, device_id=(peer, t), device_id_type=MESH)
-    pl.semaphore_wait(barrier, fs_size - 1)
-
-    def copy(q, slot):
-        return pltpu.make_async_remote_copy(
-            src_ref=part_ref.at[peers[q]], dst_ref=landed.at[slot], send_sem=send.at[q],
-            recv_sem=recv.at[q], device_id=(peers[q], t), device_id_type=MESH,
-        )
-
-    for q in range(fs_size - 1):
-        copy(q, q).start()
-    total = part_ref[f]
-    for q in range(fs_size - 1):
-        copy(q, q).wait()
-        total = total + landed[q]
-    out_ref[...] = total.astype(out_ref.dtype)
-
-
-def reduced(part):
-    fs_size, count, depth = part.shape
-    in_vmem = pl.BlockSpec(memory_space=pltpu.VMEM)
-    return pl.pallas_call(
-        reduce_kernel,
-        in_specs=[in_vmem],
-        out_specs=in_vmem,
-        out_shape=jax.ShapeDtypeStruct((count, depth), jnp.bfloat16),
-        scratch_shapes=[
-            pltpu.VMEM((fs_size - 1, count, depth), jnp.float32),
-            pltpu.SemaphoreType.DMA((fs_size - 1,)),
-            pltpu.SemaphoreType.DMA((fs_size - 1,)),
-        ],
-        compiler_params=pltpu.CompilerParams(
-            collective_id=1, has_side_effects=True, vmem_limit_bytes=REDUCE_LIMIT
-        ),
-        name="reduce_rows",
-    )(part)
 
 
 def store_kernel(joined, gate_ref, up_ref, down_ref, sems):
@@ -559,17 +526,17 @@
         out_specs=[pl.BlockSpec(memory_space=pl.ANY)] * matrices,
         out_shape=[jax.ShapeDtypeStruct((1, depth, width), joined.dtype)] * matrices,
         scratch_shapes=[pltpu.SemaphoreType.DMA((matrices, STORES))],
-        compiler_params=pltpu.CompilerParams(vmem_limit_bytes=REDUCE_LIMIT),
+        compiler_params=pltpu.CompilerParams(vmem_limit_bytes=STORE_LIMIT),
         name="store_weights",
     )(pltpu.with_memory_space_constraint(joined, pltpu.VMEM))
 
 
 def per_device(tokens, route_experts, route_logits, norm_gain, gate_train, up_train, down_train):
-    joined, _, partial = exchanged(
+    joined, _, mixed = exchanged(
         tokens, route_experts, route_logits, norm_gain, gate_train, up_train, down_train,
         lax.axis_size("fs"),
     )
-    return (*stored(joined), reduced(partial))
+    return (*stored(joined), mixed)
 
 
 def two_by_two(fs_size, tp_size, experts):

time: 345 us -> 318 us (0.922)
  Pallas kernels: 343 us -> 316 us
    pallas_call x1, Pallas kernels: 316 us -> 300 us  [exchanged(): pl.pallas_call(exchange_kernel, in_specs=[in_vmem] * 4 + [anywhere] * 3,...]
    pallas_call x1 -> x0, Pallas kernels: 10.4 us -> none  [reduced(): pl.pallas_call(reduce_kernel, in_specs=[in_vmem], out_specs=in_vmem, out_...]
where the time goes in v2:
time: 318 us; the launch traced here: 317 us
  Pallas kernels  316 us (99%)
    pallas_call x1, Pallas kernels, exchanged(): pl.pallas_call(exchange_kernel, in_specs=[in_vmem] * 4 + [anywhere] * 3,...  300 us
    pallas_call x1, Pallas kernels, stored(): pl.pallas_call(store_kernel, in_specs=[pl.BlockSpec(memory_space=pltpu.VM...  16.1 us

profile of v2, /device:TPU:0, one launch (start us, length us, event | category | flops | bytes accessed | tf_op | source)
XLA Modules:
  0.0 317.5 jit_solution(3587603352207027079)
XLA Ops:
  0.6 300.1 %exchange_weights.1 = (bf16[3,2048,4096]{2,1,0:T(8,128)(2,1)S(1)}, bf16[3,4,256,2048]{3,2,1,0:T(8,128)(2,1)}, bf16[2,2048]{1,0:T(2,128)(2,1)}) custom-call(bf16[2,2048]{1,0:T(2,128)(2,1)} %tokens_ref.1, s32[2,2]{1,0:T(2,128)} %experts_ref.1, f32[2,2]{1,0:T(2,128)} %logits_ref.1, f32[1,256]{1,0:T(1,128)} %bitcast.1, f32[4,256,2048]{2,1,0:T(8,128)} %gate_in.1, ...), custom_call_target="tpu_custom_call" | custom-call | tf_op jit(solution)/shard_map/exchange_weights/pallas_call | solution.py:466
  300.7 0.0 copy-start
  300.8 16.1 %store_weights.1 = (bf16[1,2048,4096]{2,1,0:T(8,128)(2,1)}, bf16[1,2048,4096]{2,1,0:T(8,128)(2,1)}, bf16[1,2048,4096]{2,1,0:T(8,128)(2,1)}) custom-call(bf16[3,2048,4096]{2,1,0:T(8,128)(2,1)S(1)} %get-tuple-element.9.joined), custom_call_target="tpu_custom_call" | custom-call | tf_op jit(solution)/shard_map/store_weights/pallas_call | solution.py:523
  316.9 0.0 copy-done
  316.9 0.6 copy.12
Async XLA Ops:
  300.7 16.1 %copy-start = (bf16[2,2048]{1,0:T(2,128)(2,1)S(1)}, bf16[2,2048]{1,0:T(2,128)(2,1)}, u32[]{:S(2)}) copy-start(bf16[2,2048]{1,0:T(2,128)(2,1)} %get-tuple-element.21) | copy-start | bytes 24580

commit v3 on v2

--- a/solution.py
+++ b/solution.py
@@ -11,9 +11,10 @@
 PARTS = 8
 LAG_Y = 2
 LAG_X = 5
-PER_STEP = 2
+PER_STEP = 1
 SLOTS = 4
-TILE = 512
+TILE = 1024
+SUB = 4
 VMEM_LIMIT = 16400000
 STORES = 4
 STORE_LIMIT = 2000000
@@ -104,7 +105,7 @@
     served, transit, mixed_ref,
     part_ref, landed, src, staged, scale, all_ref, acts, hidden_ref,
     l_in, z_s, z_r, y_s, y_r, x_s, x_r, c_s, c_r, g_s, g_r,
-    p_s, p_r
+    p_s, p_r, zt_r, yt_r, xt_r
 ):
     trained = (gate_in, up_in, down_in)
     matrices = len(trained)
@@ -172,14 +173,18 @@
             all_ref.at[f], all_ref.at[owner], g_s.at[q], g_r.at[q], fs_peers[q]
         )
 
-    def final(m, zs, xs, h):
-        row = pl.multiple_of((zs * 2 + xs) * rows + h * chunk, chunk)
+    def span(start, u):
+        size = chunk if u is None else chunk // SUB
+        return pl.ds(pl.multiple_of(start + (0 if u is None else u * size), size), size)
+
+    def final(m, zs, xs, h, u=None):
         return served.at[
-            m, pl.ds(row, chunk), pl.ds(pl.multiple_of(c * width, width), width)
+            m, span((zs * 2 + xs) * rows + h * chunk, u),
+            pl.ds(pl.multiple_of(c * width, width), width),
         ]
 
-    def part_of(array, m, e, h):
-        return array.at[m, e, pl.ds(pl.multiple_of(h * chunk, chunk), chunk)]
+    def part_of(array, m, e, h, u=None):
+        return array.at[m, e, span(h * chunk, u)]
 
     def source_z(j):
         return jnp.where(j == 0, z, jnp.where(j == 1, near, jnp.where(j == 2, beyond, across)))
@@ -210,35 +215,67 @@
         for n in range(matrices):
             pl.when(m == n)(functools.partial(body, n))
 
-    def send_z(m, h, e):
+    def send_z(m, h, e, u=None):
         k = z * group + m * PARTS + h
+        recv = z_r.at[k] if u is None else zt_r.at[u]
         peer = (e * 2 + x, t)
 
-        def go(here):
-            remote(part_of(src, m, e, h), here, z_s.at[e * matrices + m], z_r.at[k], peer).start()
-
-        pl.when(s == x)(lambda: go(final(m, z, x, h)))
-        pl.when(s != x)(lambda: go(part_of(transit, m, z, h)))
-
-    def send_c(m, j, zs, xs, h, q):
-        here = final(m, zs, xs, h)
+        def go(there):
+            remote(part_of(src, m, e, h, u), there, z_s.at[e * matrices + m], recv, peer).start()
+
+        pl.when(s == x)(lambda: go(final(m, z, x, h, u)))
+        pl.when(s != x)(lambda: go(part_of(transit, m, z, h, u)))
+
+    def send_c(m, j, zs, xs, h, q, u=None):
+        here = final(m, zs, xs, h, u)
         n = (j * matrices + m) * 2 + q
         remote(here, here, c_s.at[n], c_r.at[n], c_peer).start()
 
     def run(home):
-        def spread(m, j, zs, h, own):
+        def spread(m, j, zs, h, own, u=None):
             k = j * group + m * PARTS + h
             n = j * matrices + m
+            y_recv, x_recv = (y_r.at[k], x_r.at[k]) if u is None else (yt_r.at[u], xt_r.at[u])
             if home:
-                here = final(m, zs, x, h)
-                remote(here, here, y_s.at[n], y_r.at[k], y_peer).start()
-                send_c(m, j, zs, x, h, 0)
+                here = final(m, zs, x, h, u)
+                remote(here, here, y_s.at[n], y_recv, y_peer).start()
+                send_c(m, j, zs, x, h, 0, u)
             else:
-                here = part_of(src if own else transit, m, zs, h)
+                here = part_of(src if own else transit, m, zs, h, u)
                 remote(
-                    here, part_of(transit, m, zs, h), y_s.at[n], y_r.at[k], y_peer
+                    here, part_of(transit, m, zs, h, u), y_s.at[n], y_recv, y_peer
                 ).start()
-                remote(here, final(m, zs, x, h), x_s.at[n], x_r.at[k], x_peer).start()
+                remote(here, final(m, zs, x, h, u), x_s.at[n], x_recv, x_peer).start()
+
+        def from_z(k, u=None):
+            j, m, h, zs = entry(k)
+            whole = part_of(transit, 0, 0, 0, u)
+            recv = z_r.at[zs * group + m * PARTS + h] if u is None else zt_r.at[u]
+            remote(whole, whole, z_s.at[0], recv, x_peer).wait_recv()
+            spread(m, j, zs, h, False, u)
+
+        def from_y(k, u=None):
+            j, m, h, zs = entry(k)
+            n = j * group + m * PARTS + h
+            whole = part_of(transit, 0, 0, 0, u)
+            recv = y_r.at[n] if u is None else yt_r.at[u]
+            remote(whole, whole, y_s.at[0], recv, y_peer).wait_recv()
+            if home:
+                recv = x_r.at[n] if u is None else xt_r.at[u]
+                remote(
+                    part_of(transit, m, zs, h, u), final(m, zs, x, h, u),
+                    x_s.at[j * matrices + m], recv, x_peer,
+                ).start()
+            else:
+                send_c(m, j, zs, x, h, 0, u)
+
+        def from_x(k, u=None):
+            j, m, h, zs = entry(k)
+            n = j * group + m * PARTS + h
+            whole = part_of(transit, 0, 0, 0, u)
+            recv = x_r.at[n] if u is None else xt_r.at[u]
+            remote(whole, whole, x_s.at[0], recv, x_peer).wait_recv()
+            send_c(m, j, zs, 1 - x, h, 1, u)
 
         def round_group(m, g):
             h = lax.rem(g, PARTS)
@@ -273,8 +310,20 @@
 
             @pl.when(jnp.logical_not(outer))
             def _():
-                for e in far:
-                    send_z(m, h, e)
+                if m < matrices - 1:
+                    for e in far:
+                        send_z(m, h, e)
+                else:
+                    @pl.when(h < PARTS - 1)
+                    def _():
+                        for e in far:
+                            send_z(m, h, e)
+
+                    @pl.when(h == PARTS - 1)
+                    def _():
+                        for e in far:
+                            for u in range(SUB):
+                                send_z(m, h, e, u)
 
         def gate_up(m, j):
             zs = source_z(j)
@@ -318,7 +367,7 @@
 
         acts[...] = jnp.zeros_like(acts)
         rounds = group // PER_STEP
-        behind = LAG_X + 2
+        behind = LAG_X + 1
         first = 2 * group + early
         ready = first + lead + 2 * (2 * PARTS - early) + behind
         duties = (
@@ -332,8 +381,11 @@
             (ready, 1, 3),
         )
 
-        @pl.loop(0, total + LAG_X)
+        @pl.loop(0, total - 1)
         def _(i):
+            pl.when(i >= LAG_Y)(lambda: from_y(i - LAG_Y))
+            pl.when(i >= LAG_X)(lambda: from_x(i - LAG_X))
+
             @pl.when(i < rounds)
             def _():
                 for u in range(PER_STEP):
@@ -345,48 +397,13 @@
                 for q in range(fs_size - 1):
                     row_copy(q, f).start()
 
-            @pl.when((i >= LAG_Y) & (i < total + LAG_Y))
-            def _():
-                k = i - LAG_Y
-                j, m, h, zs = entry(k)
-                k = j * group + m * PARTS + h
-                whole = part_of(transit, 0, 0, 0)
-                remote(whole, whole, y_s.at[0], y_r.at[k], y_peer).wait_recv()
-
-                def go(m):
-                    if home:
-                        remote(
-                            part_of(transit, m, zs, h), final(m, zs, x, h),
-                            x_s.at[j * matrices + m], x_r.at[k], x_peer,
-                        ).start()
-                    else:
-                        send_c(m, j, zs, x, h, 0)
-
-                go(m)
-
-            @pl.when(i >= LAG_X)
-            def _():
-                k = i - LAG_X
-                j, m, h, zs = entry(k)
-                k = j * group + m * PARTS + h
-                whole = part_of(transit, 0, 0, 0)
-                remote(whole, whole, x_s.at[0], x_r.at[k], x_peer).wait_recv()
-                send_c(m, j, zs, 1 - x, h, 1)
-
             @pl.when(outer & (i >= rounds) & (i < rounds + group))
             def _():
                 g = i - rounds
                 for e in far:
                     send_z(lax.div(g, PARTS), lax.rem(g, PARTS), e)
 
-            @pl.when((i >= group) & (i < total))
-            def _():
-                j, m, h, zs = entry(i)
-                whole = part_of(transit, 0, 0, 0)
-                remote(
-                    whole, whole, z_s.at[0], z_r.at[zs * group + m * PARTS + h], x_peer
-                ).wait_recv()
-                spread(m, j, zs, h, False)
+            pl.when(i >= group)(lambda: from_z(i))
 
             @pl.when(i == group)
             def _():
@@ -419,10 +436,29 @@
                         weight * jax.nn.silu(gate_act) * up_act
                     ).astype(jnp.bfloat16)
 
-            @pl.when((i > ready + 1) & (i < ready + 1 + experts))
-            def _():
-                mix(i - ready - 2)
-
+            @pl.when(i == ready + 2)
+            def _():
+                mix(0)
+
+        last = total - 1
+        for k in range(last - LAG_Y, last - 1):
+            from_y(k)
+        for k in range(last - LAG_X, last - 2):
+            from_x(k)
+        tail = [(from_z, last, u) for u in range(SUB)]
+        tail[SUB // 2:SUB // 2] = [(from_y, last - 1, None), (from_x, last - 2, None)]
+        tail.append((from_x, last - 1, None))
+        for u in range(SUB):
+            tail.append((from_y, last, u))
+            if u:
+                tail.append((from_x, last, u - 1))
+        tail.append((from_x, last, SUB - 1))
+        for n, (step, k, u) in enumerate(tail):
+            if n == SUB + 2:
+                mix(1)
+            if n == SUB + 5:
+                mix(2)
+            step(k, u)
         mix(experts - 1)
 
         def part_copy(q):
@@ -494,6 +530,9 @@
             dma((fs_size - 1,)),
             dma((fs_size - 1,)),
             dma((fs_size - 1,)),
+            dma((SUB,)),
+            dma((SUB,)),
+            dma((SUB,)),
         ],
         compiler_params=pltpu.CompilerParams(
             collective_id=0, has_side_effects=True, vmem_limit_bytes=VMEM_LIMIT

time: 318 us -> 318 us (level)
  no operation moved by 1% of the time
where the time goes in v3:
time: 318 us
  Pallas kernels  316 us (99%)
    pallas_call x1, Pallas kernels, exchanged(): pl.pallas_call(exchange_kernel, in_specs=[in_vmem] * 4 + [anywhere] * 3,...  300 us
    pallas_call x1, Pallas kernels, stored(): pl.pallas_call(store_kernel, in_specs=[pl.BlockSpec(memory_space=pltpu.VM...  16.1 us

profile of v3, /device:TPU:0, one launch (start us, length us, event | category | flops | bytes accessed | tf_op | source)
XLA Modules:
  0.0 317.6 jit_solution(9496817659725246316)
XLA Ops:
  0.6 300.2 %exchange_weights.1 = (bf16[3,2048,4096]{2,1,0:T(8,128)(2,1)S(1)}, bf16[3,4,256,2048]{3,2,1,0:T(8,128)(2,1)}, bf16[2,2048]{1,0:T(2,128)(2,1)}) custom-call(bf16[2,2048]{1,0:T(2,128)(2,1)} %tokens_ref.1, s32[2,2]{1,0:T(2,128)} %experts_ref.1, f32[2,2]{1,0:T(2,128)} %logits_ref.1, f32[1,256]{1,0:T(1,128)} %bitcast.1, f32[4,256,2048]{2,1,0:T(8,128)} %gate_in.1, ...), custom_call_target="tpu_custom_call" | custom-call | tf_op jit(solution)/shard_map/exchange_weights/pallas_call | solution.py:502
  300.8 0.0 copy-start
  300.9 16.1 %store_weights.1 = (bf16[1,2048,4096]{2,1,0:T(8,128)(2,1)}, bf16[1,2048,4096]{2,1,0:T(8,128)(2,1)}, bf16[1,2048,4096]{2,1,0:T(8,128)(2,1)}) custom-call(bf16[3,2048,4096]{2,1,0:T(8,128)(2,1)S(1)} %get-tuple-element.9.joined), custom_call_target="tpu_custom_call" | custom-call | tf_op jit(solution)/shard_map/store_weights/pallas_call | solution.py:562
  317.0 0.0 copy-done
  317.0 0.6 copy.12
Async XLA Ops:
  300.8 16.1 %copy-start = (bf16[2,2048]{1,0:T(2,128)(2,1)S(1)}, bf16[2,2048]{1,0:T(2,128)(2,1)}, u32[]{:S(2)}) copy-start(bf16[2,2048]{1,0:T(2,128)(2,1)} %get-tuple-element.21) | copy-start | bytes 24580
